TPU v7x, 32 devices: a whole 2x2x4 slice. The times are simulated.
32 devices in a mesh: sp: 8 (over z, x), tp: 4 (over y, core).
Axes of the slice: x: 2, y: 2, z: 4, core: 2. Of those that a mesh axis runs over, the one named last changes fastest.
Arguments:
- resid: bfloat16 [2048, 2048], P('sp'), may hold values from -6 to 6
- query_one: bfloat16 [2048, 1024], P('sp', 'tp'), may hold values from -400 to 400
- query_two: bfloat16 [2048, 1024], P('sp', 'tp'), may hold values from -400 to 400
- key_one: bfloat16 [2048, 1024], P('sp', 'tp'), may hold values from -8 to 8
- key_two: bfloat16 [2048, 1024], P('sp', 'tp'), may hold values from -8 to 8
- values: bfloat16 [2048, 2048], P('sp', 'tp'), may hold values from -6 to 6
- documents: int32 [2048], P('sp'), may hold values from 0 to 1, never falling along the last dimension, each value on 1 to 1280 neighbouring positions
- mix_lambda: float32 [16], P('tp'), may hold values from 0.3 to 0.8
- head_gain: float32 [128], replicated, may hold values from 0.1 to 1.9
- out_weight: bfloat16 [2048, 2048], P('tp'), may hold values from -0.125 to 0.125
- ffn_gain: float32 [2048], replicated, may hold values from 0.1 to 1.9
- routes: int32 [2048, 4], P('sp'), may hold values from 0 to 31, all different within a row; in each aligned block of 256 rows (0 to 255, 256 to 511, ...) at most 64 rows name the same one
- route_weight: float32 [2048, 4], P('sp'), may hold values from 0.2 to 0.9
- expert_gate: bfloat16 [32, 2048, 512], P(('sp', 'tp')), may hold values from -0.125 to 0.125
- expert_up: bfloat16 [32, 2048, 512], P(('sp', 'tp')), may hold values from -0.125 to 0.125
- expert_down: bfloat16 [32, 512, 2048], P(('sp', 'tp')), may hold values from -0.25 to 0.25
- shared_gate: bfloat16 [2048, 512], P(None, 'tp'), may hold values from -0.125 to 0.125
- shared_up: bfloat16 [2048, 512], P(None, 'tp'), may hold values from -0.125 to 0.125
- shared_down: bfloat16 [512, 2048], P('tp'), may hold values from -0.25 to 0.25
Outputs:
- layer_out: bfloat16 [2048, 2048], P(('sp', 'tp'))
Inputs may be any that keep to these rules, and one draw needn't show every extreme that they name: `documents`: document numbers never fall along the positions; each document has 1 to 1280 positions and one has exactly 1280. `routes`: A row names 4 different experts. In each aligned block of 256 rows no expert is named by more than 64 rows, a bound that some block reaches.
All inputs are finite; a program needn't handle non-finite values.
Results may differ from a plain program's by a relative error of at most 0.018.
Values may be sent and summed in bfloat16 or wider, within the bound.
A program may use at most 128 MiB of HBM per device.

v0:
```python
import jax
import jax.numpy as jnp
from jax import lax
from jax.sharding import PartitionSpec as P

NEG_FILL = -1e30
HEAD_SCALE = 0.8


def rms_scale(values_in, eps_value):
    return lax.rsqrt(jnp.mean(values_in * values_in, axis=-1, keepdims=True) + eps_value)


def local(
    resid,
    query_one,
    query_two,
    key_one,
    key_two,
    values,
    documents,
    mix_lambda,
    head_gain,
    out_weight,
    ffn_gain,
    routes,
    route_weight,
    expert_gate,
    expert_up,
    expert_down,
    shared_gate,
    shared_up,
    shared_down,
):
    tok_rows = query_one.shape[0]
    head_count = mix_lambda.shape[0]
    head_width = query_one.shape[1] // head_count
    value_width = values.shape[1] // head_count
    model_width = resid.shape[1]
    score_scale = head_width ** (-0.5)
    seq_size = lax.axis_size("sp")
    tp_size = lax.axis_size("tp")
    query_pos = lax.axis_index("sp") * tok_rows + jnp.arange(tok_rows, dtype=jnp.int32)
    query_first = query_one.reshape(tok_rows, head_count, head_width)
    query_second = query_two.reshape(tok_rows, head_count, head_width)
    lambda_col = mix_lambda[:, None, None]
    first_doc = documents[0]
    last_pos = query_pos[tok_rows - 1]

    def masks(key_docs):
        key_pos = jnp.arange(key_docs.shape[0], dtype=jnp.int32)
        return (
            (key_pos[None, :] <= query_pos[:, None]) & (key_docs[None, :] == documents[:, None])
        )[None]

    def needed(key_docs, offset):
        return (offset <= last_pos) & (jnp.max(key_docs) >= first_doc)

    def scores(query_block, key_block):
        keyed = key_block.reshape(key_block.shape[0], head_count, head_width)
        return (
            jnp.einsum("qhd,khd->hqk", query_block, keyed, preferred_element_type=jnp.float32)
            * score_scale
        )

    empty_max = jnp.full((head_count, tok_rows), NEG_FILL, jnp.float32)
    empty_sum = jnp.zeros((head_count, tok_rows), jnp.float32)
    stats_init = ((empty_max, empty_sum), (empty_max, empty_sum))
    value_init = jnp.zeros((head_count, tok_rows, value_width), jnp.float32)
    key_first = lax.all_gather(key_one, "sp", axis=0, tiled=True)
    key_second = lax.all_gather(key_two, "sp", axis=0, tiled=True)
    key_docs = lax.all_gather(documents, "sp", axis=0, tiled=True)

    def stats_update(current):
        allowed = masks(key_docs)
        result = []
        for query_block, key_block, (top_now, sum_now) in (
            (query_first, key_first, current[0]),
            (query_second, key_second, current[1]),
        ):
            masked = jnp.where(allowed, scores(query_block, key_block), NEG_FILL)
            top_next = jnp.maximum(top_now, jnp.max(masked, axis=-1))
            fresh = jnp.where(allowed, jnp.exp(masked - top_next[:, :, None]), 0.0)
            result.append((top_next, jnp.sum(fresh, axis=-1)))
        return tuple(result)

    def stats_keep(current):
        return current

    soft_stats = lax.cond(needed(key_docs, jnp.int32(0)), stats_update, stats_keep, stats_init)
    apply_key_first = lax.all_gather(key_one, "sp", axis=0, tiled=True)
    apply_key_second = lax.all_gather(key_two, "sp", axis=0, tiled=True)
    value_block = lax.all_gather(values, "sp", axis=0, tiled=True)
    apply_key_docs = lax.all_gather(documents, "sp", axis=0, tiled=True)

    def apply_update(current):
        allowed = masks(apply_key_docs)
        probs = []
        for query_block, key_block, (top_all, sum_all) in (
            (query_first, apply_key_first, soft_stats[0]),
            (query_second, apply_key_second, soft_stats[1]),
        ):
            raw = scores(query_block, key_block)
            probs.append(
                jnp.where(allowed, jnp.exp(raw - top_all[:, :, None]), 0.0) / sum_all[:, :, None]
            )
        weights = (probs[0] - lambda_col * probs[1]).astype(jnp.bfloat16)
        valued = value_block.reshape(value_block.shape[0], head_count, value_width)
        return current + jnp.einsum(
            "hqk,khv->hqv", weights, valued, preferred_element_type=jnp.float32
        )

    def apply_keep(current):
        return current

    head_out = lax.cond(needed(apply_key_docs, jnp.int32(0)), apply_update, apply_keep, value_init)
    normed_heads = (head_out * rms_scale(head_out, 1e-05) * head_gain * HEAD_SCALE).astype(
        jnp.bfloat16
    )
    attn_rows = normed_heads.transpose(1, 0, 2).reshape(tok_rows, head_count * value_width)
    share_rows = tok_rows // tp_size
    own_start = lax.axis_index("tp") * share_rows
    proj_term = jnp.dot(attn_rows, out_weight, preferred_element_type=jnp.float32)
    projected = lax.psum(proj_term.astype(jnp.bfloat16), "tp").astype(jnp.float32)
    mixed_all = resid.astype(jnp.float32) + projected
    normed_all = (mixed_all * rms_scale(mixed_all, 1e-06) * ffn_gain).astype(jnp.bfloat16)
    mixed_own = lax.dynamic_slice_in_dim(mixed_all, own_start, share_rows, 0)
    route_slots = routes.shape[1]
    capacity = max(2, 2 * tok_rows * route_slots // (seq_size * tp_size))
    assign_total = tok_rows * route_slots
    flat_expert = routes.reshape(assign_total)
    flat_weight = route_weight.reshape(assign_total)
    assign_token = jnp.arange(assign_total, dtype=jnp.int32) // route_slots
    is_mine = flat_expert % tp_size == lax.axis_index("tp")
    target = flat_expert // tp_size
    one_hot = (
        (target[:, None] == jnp.arange(seq_size, dtype=jnp.int32)[None, :]) & is_mine[:, None]
    ).astype(jnp.int32)
    slot_rank = jnp.sum(jnp.cumsum(one_hot, axis=0) * one_hot, axis=1) - 1
    slot_id = jnp.where(is_mine, target * capacity + slot_rank, -1)
    slot_total = seq_size * capacity
    matches = slot_id[None, :] == jnp.arange(slot_total, dtype=jnp.int32)[:, None]
    slot_token = jnp.sum(jnp.where(matches, assign_token[None, :], 0), axis=1)
    slot_live = jnp.any(matches, axis=1)
    outgoing = jnp.where(
        slot_live[:, None], normed_all[slot_token], jnp.zeros((), jnp.bfloat16)
    ).reshape(seq_size, capacity, model_width)
    arrived = lax.all_to_all(outgoing, "sp", split_axis=0, concat_axis=0, tiled=True)
    item_count = arrived.shape[1]
    flat_rows = arrived.reshape(seq_size * item_count, model_width)
    gate_part = jnp.dot(flat_rows, expert_gate[0], preferred_element_type=jnp.float32)
    up_part = jnp.dot(flat_rows, expert_up[0], preferred_element_type=jnp.float32)
    hidden = (jax.nn.silu(gate_part) * up_part).astype(jnp.bfloat16)
    result = jnp.dot(hidden, expert_down[0], preferred_element_type=jnp.float32).astype(
        jnp.bfloat16
    )
    returned = lax.all_to_all(
        result.reshape(seq_size, item_count, model_width),
        "sp",
        split_axis=0,
        concat_axis=0,
        tiled=True,
    )
    returned_flat = returned.reshape(slot_total, model_width)
    picked = returned_flat[jnp.maximum(slot_id, 0)].astype(jnp.float32)
    picked_weight = jnp.where(is_mine, flat_weight, 0.0)
    routed = jnp.sum(
        (picked * picked_weight[:, None]).reshape(tok_rows, route_slots, model_width), axis=1
    )
    shared_act = (
        jax.nn.silu(jnp.dot(normed_all, shared_gate, preferred_element_type=jnp.float32))
        * jnp.dot(normed_all, shared_up, preferred_element_type=jnp.float32)
    ).astype(jnp.bfloat16)
    shared_out = jnp.dot(shared_act, shared_down, preferred_element_type=jnp.float32)
    ffn_own = lax.psum_scatter(
        (routed + shared_out).astype(jnp.bfloat16), "tp", scatter_dimension=0, tiled=True
    ).astype(jnp.float32)
    return (mixed_own + ffn_own).astype(jnp.bfloat16)


def solution(mesh):
    placed = (
        P("sp", None),
        P("sp", "tp"),
        P("sp", "tp"),
        P("sp", "tp"),
        P("sp", "tp"),
        P("sp", "tp"),
        P("sp"),
        P("tp"),
        P(),
        P("tp", None),
        P(),
        P("sp", None),
        P("sp", None),
        P(("sp", "tp"), None, None),
        P(("sp", "tp"), None, None),
        P(("sp", "tp"), None, None),
        P(None, "tp"),
        P(None, "tp"),
        P("tp", None),
    )
    return jax.shard_map(
        local, mesh=mesh, in_specs=placed, out_specs=P(("sp", "tp"), None), check_vma=False
    )
```

profile of v0, /device:TPU:0, one launch (start us, length us, event | category | flops | bytes accessed | tf_op | source)
XLA Modules:
  0.0 388.5 jit_solution(5894218725486632129)
XLA Ops:
  6.5 1.8 copy.47
  8.4 1.7 copy.49
  10.2 1.8 copy.51
  15.9 22.3 %all-gather = s32[8,1,256]{2,1,0:T(1,128)S(1)} all-gather(s32[1,1,256]{2,1,0:T(1,128)S(1)} %bitcast.92), channel_id=1, replica_groups=mesh['sp'=8,'tp'=4] {'sp'}, dimensions={0}, use_global_device_ids=true | all-gather | bytes 9216 | tf_op jit(solution)/shard_map/all_gather | solution.py:94
  40.0 2.3 reduce-window.6
  42.9 8.6 %all-gather.5.cloned.1.call-done = bf16[2048,256]{0,1:T(8,128)(2,1)} async-done(((bf16[256,256]{0,1:T(8,128)(2,1)}), bf16[2048,256]{0,1:T(8,128)(2,1)}) %all-gather.5.cloned.1.call-update) | async-done | bytes 1048592 | tf_op jit(solution)/shard_map/all_gather | solution.py:91
  51.6 40.5 %all-gather.7.cloned.1.call-done = bf16[2048,256]{0,1:T(8,128)(2,1)} async-done(((bf16[256,256]{0,1:T(8,128)(2,1)}), bf16[2048,256]{0,1:T(8,128)(2,1)}) %all-gather.7.cloned.1.call-update) | async-done | bytes 1048592 | tf_op jit(solution)/shard_map/all_gather | solution.py:71
  92.0 12.4 %conditional.2 = (f32[4,256]{1,0:T(4,128)}, f32[4,256]{1,0:T(4,128)S(1)}, f32[4,256]{1,0:T(4,128)}, f32[4,256]{1,0:T(4,128)S(1)}) conditional(s32[]{:T(128)} %convert_element_type.53, () %tuple.24, (s32[256]{0:T(256)S(1)}, s32[2048]{0:T(1024)S(1)}, s32[256]{0:T(256)S(1)}, bf16[2048,256]{0,1:T(8,128)(2,1)}, bf16[256,4,64]{0,2,1:T(8,128)(2,1)S(1)}, ...), branch_computations={%region_1.0_spmd, %region_2.7_spmd} | conditional | flops 571996160 | bytes 50120764 | solution.py:90
  92.0 2.6 fusion.55
  95.2 3.1 fusion.1
  98.9 5.5 %select_reduce_fusion = (f32[4,256]{1,0:T(4,128)S(1)}, f32[4,256]{1,0:T(4,128)S(1)}) fusion(f32[4,256,2048]{2,1,0:T(8,128)S(1)} %get-tuple-element.106, f32[4,256]{1,0:T(4,128)} %get-tuple-element.122, pred[256,2048]{1,0:T(8,128)(4,1)S(1)} %fusion.2, f32[4,256]{1,0:T(4,128)} %get-tuple-element.120, f32[4,256,2048]{2,1,0:T(8,128)S(1)} %fusion.55), kind=kLoop, calls=%fused_computation.2 | loop fusion | flops 20969472 | bytes 17317888 | tf_op jit(solution)/shard_map/cond/branch_1_fun/reduce_sum | solution.py:84
  104.4 39.0 %all-gather.9.cloned.1.call-done = bf16[2048,512]{0,1:T(8,128)(2,1)} async-done(((bf16[256,512]{0,1:T(8,128)(2,1)}), bf16[2048,512]{0,1:T(8,128)(2,1)}) %all-gather.9.cloned.1.call-update) | async-done | bytes 2097168 | tf_op jit(solution)/shard_map/all_gather | solution.py:93
  143.5 16.7 %conditional.3 = (f32[4,256,128]{1,2,0:T(8,128)S(1)}, f32[4,256,1]{1,0,2:T(4,128)S(1)}) conditional(s32[]{:T(128)} %convert_element_type.53, () %tuple.23, (s32[256]{0:T(256)S(1)}, s32[2048]{0:T(1024)S(1)}, s32[256]{0:T(256)S(1)}, bf16[2048,256]{0,1:T(8,128)(2,1)}, bf16[256,4,64]{0,2,1:T(8,128)(2,1)S(1)}, /*index=5*/f32[4,256]{1,0:T(4,128)}, ...), branch_computations={%region_7.8_spmd, %region_8.0_spmd} | conditional | flops 1098644480 | bytes 22837280 | solution.py:116
  143.5 5.7 %fusion.56 = f32[4,256,2048]{2,1,0:T(8,128)} fusion(bf16[256,4,64]{0,2,1:T(8,128)(2,1)S(1)} %get-tuple-element.58, bf16[2048,4,64]{0,2,1:T(8,128)(2,1)} %bitcast.75), kind=kOutput, calls=%fused_computation.113 | convolution fusion | flops 268435456 | bytes 9568256 | tf_op jit(solution)/shard_map/cond/branch_1_fun/qhd,khd->hqk/dot_general | solution.py:62
  150.6 9.6 %multiply_reduce_fusion = (f32[4,256]{1,0:T(4,128)S(1)}, f32[4,256,128]{1,2,0:T(8,128)S(1)}) fusion(bf16[2048,4,128]{0,2,1:T(8,128)(2,1)} %bitcast.95, f32[4,256,2048]{2,1,0:T(8,128)} %fusion.56, bf16[256,4,64]{0,2,1:T(8,128)(2,1)S(1)} %get-tuple-element.63, bf16[2048,4,64]{0,2,1:T(8,128)(2,1)} %bitcast.82, f32[4,256]{1,0:T(4,128)S(1)} %get-tuple-element.66, ...), kind=kOutput, calls=%fused_computation.21 | convolution fusion | flops 828636160 | bytes 12734480 | tf_op jit(solution)/shard_map/cond/branch_1_fun/hqk,khv->hqv/dot_general | solution.py:109
  160.4 3.4 convolution_convert_fusion.1
  164.6 33.9 %all-reduce.2.cloned.1.call-done = bf16[256,2048]{1,0:T(8,128)(2,1)} async-done(((bf16[256,2048]{1,0:T(8,128)(2,1)}), bf16[256,2048]{1,0:T(8,128)(2,1)}) %all-reduce.2.cloned.1.call-update) | async-done | bytes 1048592 | tf_op jit(solution)/shard_map/psum | solution.py:124
  198.5 3.1 convert_add_fusion
  202.2 3.3 gather_fusion
  205.5 1.8 broadcast_select_fusion
  207.3 53.2 %all_to_all.10 = bf16[8,64,2048]{2,1,0:T(8,128)(2,1)S(1)} all-to-all(bf16[8,64,2048]{2,1,0:T(8,128)(2,1)S(1)} %broadcast_select_fusion), channel_id=1, replica_groups=mesh['sp'=8,'tp'=4] {'sp'}, dimensions={0} | all-to-all | bytes 4194304 | tf_op jit(solution)/shard_map/all_to_all | solution.py:148
  261.8 2.2 fusion.16
  264.1 6.3 %convolution_convert_fusion = bf16[512,2048]{1,0:T(8,128)(2,1)} fusion(bf16[1,512,2048]{2,1,0:T(8,128)(2,1)S(1)} %copy-done, bf16[512,2048]{1,0:T(8,128)(2,1)} %bitcast.78, bf16[1,2048,512]{2,1,0:T(8,128)(2,1)} %param.37, f32[512,512]{1,0:T(8,128)} %fusion.16), kind=kOutput, calls=%fused_computation.25 | convolution fusion | flops 2150105088 | bytes 9437184 | tf_op jit(solution)/shard_map/dot_general | solution.py:154
  270.3 4.5 %all-to-all-start.1 = ((bf16[8,64,2048]{2,1,0:T(8,128)(2,1)}), bf16[8,64,2048]{2,1,0:T(8,128)(2,1)}, u32[]{:S(2)}, u32[]{:S(2)}) async-start(bf16[8,64,2048]{2,1,0:T(8,128)(2,1)} %bitcast.76), calls=%async_computation.1 | async-start | bytes 4194304 | tf_op jit(solution)/shard_map/all_to_all | solution.py:157
  275.3 1.5 fusion.57
  276.7 45.4 %all-to-all-done.1 = bf16[8,64,2048]{2,1,0:T(8,128)(2,1)} async-done(((bf16[8,64,2048]{2,1,0:T(8,128)(2,1)}), bf16[8,64,2048]{2,1,0:T(8,128)(2,1)}, u32[]{:S(2)}, u32[]{:S(2)}) %all-to-all-start.1) | async-done | bytes 2097184 | tf_op jit(solution)/shard_map/all_to_all | solution.py:157
  322.1 10.7 %gather_fusion.1 = bf16[1024,2048]{1,0:T(8,128)(2,1)} fusion(bf16[512,2048]{1,0:T(8,128)(2,1)} %bitcast.24, s32[1024]{0:T(1024)S(1)} %broadcast_clamp_fusion), kind=kCustom, calls=%fused_computation.1 | custom fusion | bytes 8392704 | tf_op jit(solution)/shard_map/gather | solution.py:165
  332.8 8.3 %reshape.441 = f32[256,4,2048]{2,1,0:T(4,128)} reshape(bf16[1024,2048]{1,0:T(8,128)(2,1)} %gather_fusion.1) | data formatting | bytes 12582912 | tf_op jit(solution)/shard_map/convert_element_type | solution.py:165
  341.1 11.4 %multiply_reduce_fusion.1 = f32[256,2048]{1,0:T(8,128)} fusion(f32[256,4,2048]{2,1,0:T(4,128)} %reshape.441, f32[256,4]{1,0:T(8,128)S(1)} %copy.55), kind=kLoop, calls=%fused_computation.24 | loop fusion | flops 3670016 | bytes 10489856 | tf_op jit(solution)/shard_map/reduce_sum | solution.py:167
  352.5 3.7 fusion.12
  356.2 23.9 %reduce-scatter.2.cloned.1.call-done = bf16[64,2048]{1,0:T(8,128)(2,1)} async-done(((bf16[256,2048]{1,0:T(8,128)(2,1)}), bf16[64,2048]{1,0:T(8,128)(2,1)}) %reduce-scatter.2.cloned.1.call-update) | async-done | bytes 262160 | tf_op jit(solution)/shard_map/reduce_scatter | solution.py:175
  380.1 1.9 add_convert_fusion
  (74 shorter events, 10.3 us)
Async XLA Ops:
  6.5 257.5 %copy-start = (bf16[1,512,2048]{2,1,0:T(8,128)(2,1)S(1)}, bf16[1,512,2048]{2,1,0:T(8,128)(2,1)}, u32[]{:S(2)}) copy-start(bf16[1,512,2048]{2,1,0:T(8,128)(2,1)} %param.38) | copy-start | bytes 6291460
  6.5 7.6 %copy-start.6 = (bf16[256,256]{1,0:T(8,128)(2,1)S(1)}, bf16[256,256]{1,0:T(8,128)(2,1)}, u32[]{:S(2)}) copy-start(bf16[256,256]{1,0:T(8,128)(2,1)} %param.25) | copy-start | bytes 393220
  6.5 8.3 %copy-start.8 = (s32[256]{0:T(256)S(1)}, s32[256]{0:T(256)}, u32[]{:S(2)}) copy-start(s32[256]{0:T(256)} %param.29) | copy-start | bytes 3076
  6.5 45.0 %all-gather.5.cloned.1.call-start = ((), (), s32[]{:S(2)}) async-start(), calls=%async_computation.3 | async-start | bytes 1179648 | tf_op jit(solution)/shard_map/all_gather | solution.py:91
  8.4 83.7 %all-gather.7.cloned.1.call-start = ((), (), s32[]{:S(2)}) async-start(), calls=%async_computation.4 | async-start | bytes 1179648 | tf_op jit(solution)/shard_map/all_gather | solution.py:71
  10.1 133.4 %all-gather.9.cloned.1.call-start = ((), (), s32[]{:S(2)}) async-start(), calls=%async_computation.5 | async-start | bytes 2359296 | tf_op jit(solution)/shard_map/all_gather | solution.py:93
  12.0 186.5 %all-reduce.2.cloned.1.call-start = ((), (), s32[]{:S(2)}) async-start(), calls=%async_computation.6 | async-start | bytes 2097152 | tf_op jit(solution)/shard_map/psum | solution.py:124
  92.0 51.5 %copy-start.13 = (f32[4]{0:T(128)S(1)}, f32[4]{0:T(128)}, u32[]{:S(2)}) copy-start(f32[4]{0:T(128)} %param.30) | copy-start | bytes 52
  92.0 3.2 copy-start.5
  143.5 16.8 %copy-start.11 = (f32[128]{0:T(128)S(1)}, f32[128]{0:T(128)}, u32[]{:S(2)}) copy-start(f32[128]{0:T(128)} %param.31) | copy-start | bytes 1540
  160.4 38.1 %copy-start.1 = (bf16[256,2048]{1,0:T(8,128)(2,1)S(1)}, bf16[256,2048]{1,0:T(8,128)(2,1)}, u32[]{:S(2)}) copy-start(bf16[256,2048]{1,0:T(8,128)(2,1)} %param.23) | copy-start | bytes 3145732
  164.6 37.0 %copy-start.9 = (f32[2048]{0:T(1024)S(1)}, f32[2048]{0:T(1024)}, u32[]{:S(2)}) copy-start(f32[2048]{0:T(1024)} %param.33) | copy-start | bytes 24580
  198.5 3.1 copy-start.2
  198.5 3.1 copy-start.3
  207.3 54.5 %copy-start.12 = (bf16[1,2048,512]{2,1,0:T(8,128)(2,1)S(1)}, bf16[1,2048,512]{2,1,0:T(8,128)(2,1)}, u32[]{:S(2)}) copy-start(bf16[1,2048,512]{2,1,0:T(8,128)(2,1)} %param.36) | copy-start | bytes 6291460
  260.5 1.3 copy-start.4
  270.3 4.7 %copy-start.7 = (s32[256,4]{0,1:T(4,128)S(1)}, s32[256,4]{0,1:T(4,128)}, u32[]{:S(2)}) copy-start(s32[256,4]{0,1:T(4,128)} %param.34) | copy-start | bytes 12292
  270.3 4.7 %copy-start.10 = (f32[256,4]{0,1:T(4,128)S(1)}, f32[256,4]{0,1:T(4,128)}, u32[]{:S(2)}) copy-start(f32[256,4]{0,1:T(4,128)} %param.35) | copy-start | bytes 12292
  270.3 51.7 %all-to-all-start.1 = ((bf16[8,64,2048]{2,1,0:T(8,128)(2,1)}), bf16[8,64,2048]{2,1,0:T(8,128)(2,1)}, u32[]{:S(2)}, u32[]{:S(2)}) async-start(bf16[8,64,2048]{2,1,0:T(8,128)(2,1)} %bitcast.76), calls=%async_computation.1 | async-start | bytes 4194304 | tf_op jit(solution)/shard_map/all_to_all | solution.py:157
  274.8 105.3 %reduce-scatter.2.cloned.1.call-start = ((), (), s32[]{:S(2)}) async-start(), calls=%async_computation.7 | async-start | bytes 1310720 | tf_op jit(solution)/shard_map/reduce_scatter | solution.py:175
Sparse Core Ops, SparseCore 0:
  9.4 42.1 all-gather.4
  53.6 38.3 all-gather.6
  94.1 49.3 all-gather.8
  164.0 34.4 all-reduce.1
  356.3 23.7 reduce-scatter.1
where the time goes:
time: 389 us
  waiting for transfers between devices  191 us (49%)
  blocking collectives  75.5 us (19%)
  matrix products  38.2 us (10%)
  local copies, waits for them, and re-layouts  32.8 us (8%)
  other arithmetic  30.8 us (8%)
  between operations  15.1 us (4%)
  starting transfers between devices  4.67 us (1%)
    all_to_all x1, blocking collectives, local(): lax.all_to_all(outgoing, 'sp', split_axis=0, concat_axis=0, tiled=True)  53.2 us
    all_to_all x1, waiting for transfers between devices, local(): lax.all_to_all(result.reshape(seq_size, item_count, model_width), 'sp', s...  45.4 us
    all_gather x1, waiting for transfers between devices, local(): key_second = lax.all_gather(key_two, 'sp', axis=0, tiled=True)  40.5 us
    all_gather x1, waiting for transfers between devices, local(): value_block = lax.all_gather(values, 'sp', axis=0, tiled=True)  39 us
    psum x1, waiting for transfers between devices, local(): lax.psum(proj_term.astype(jnp.bfloat16), 'tp').astype(jnp.float32)  33.9 us
    reduce_scatter x1, waiting for transfers between devices, local(): lax.psum_scatter((routed + shared_out).astype(jnp.bfloat16), 'tp', scatte...  23.9 us
    all_gather x1, blocking collectives, local(): apply_key_docs = lax.all_gather(documents, 'sp', axis=0, tiled=True)  22.3 us
    dot_general x3, matrix products, scores(): jnp.einsum('qhd,khd->hqk', query_block, keyed, preferred_element_type=jnp...  11.5 us
  transfers between devices with their start and end apart: 6, of which 6 were waited for; matrix products, arithmetic and copies ran while one was open for 6% of the time, Pallas kernels for 0%

commit v1 on v0

--- a/solution.py
+++ b/solution.py
@@ -91,7 +91,8 @@
     apply_key_first = lax.all_gather(key_one, "sp", axis=0, tiled=True)
     apply_key_second = lax.all_gather(key_two, "sp", axis=0, tiled=True)
     value_block = lax.all_gather(values, "sp", axis=0, tiled=True)
-    apply_key_docs = lax.all_gather(documents, "sp", axis=0, tiled=True)
+    sent = jnp.stack([documents] * lax.axis_size("sp"))
+    apply_key_docs = jnp.concatenate(lax.all_to_all(sent, "sp", 0, 0), axis=0)
 
     def apply_update(current):
         allowed = masks(apply_key_docs)

time: 389 us -> 389 us (level)
  waiting for transfers between devices: 191 us -> 183 us
  starting transfers between devices: 4.67 us -> 12 us
    all_gather x1, waiting for transfers between devices: 8.64 us -> 0.11 us  [local(): apply_key_first = lax.all_gather(key_one, 'sp', axis=0, tiled=True)]
    all_to_all x0 -> x1, starting transfers between devices: none -> 7.28 us  [local(): apply_key_docs = jnp.concatenate(lax.all_to_all(sent, 'sp', 0, 0), axis=0)]
    unnamed x32 -> x34, local copies, waits for them, and re-layouts: 8.52 us -> 7.61 us
  transfers between devices with their start and end apart: 6 -> 7, of which waited for: 6 -> 6; matrix products, arithmetic and copies ran while one was open for 6% -> 7% of each run, Pallas kernels for 0% -> 0%
where the time goes in v1:
time: 389 us; the launch traced here: 388 us
  waiting for transfers between devices  183 us (47%)
  blocking collectives  74.2 us (19%)
  matrix products  38.2 us (10%)
  local copies, waits for them, and re-layouts  33.2 us (9%)
  other arithmetic  31.6 us (8%)
  between operations  16.5 us (4%)
  starting transfers between devices  12 us (3%)
    all_to_all x1, blocking collectives, local(): lax.all_to_all(outgoing, 'sp', split_axis=0, concat_axis=0, tiled=True)  53.2 us
    all_to_all x1, waiting for transfers between devices, local(): lax.all_to_all(result.reshape(seq_size, item_count, model_width), 'sp', s...  45.4 us
    all_gather x1, waiting for transfers between devices, local(): key_second = lax.all_gather(key_two, 'sp', axis=0, tiled=True)  40.3 us
    all_gather x1, waiting for transfers between devices, local(): value_block = lax.all_gather(values, 'sp', axis=0, tiled=True)  39 us
    psum x1, waiting for transfers between devices, local(): lax.psum(proj_term.astype(jnp.bfloat16), 'tp').astype(jnp.float32)  33.9 us
    reduce_scatter x1, waiting for transfers between devices, local(): lax.psum_scatter((routed + shared_out).astype(jnp.bfloat16), 'tp', scatte...  23.9 us
    all_gather x1, blocking collectives, local(): key_docs = lax.all_gather(documents, 'sp', axis=0, tiled=True)  21 us
    dot_general x3, matrix products, scores(): jnp.einsum('qhd,khd->hqk', query_block, keyed, preferred_element_type=jnp...  11.5 us
  transfers between devices with their start and end apart: 7, of which 6 were waited for; matrix products, arithmetic and copies ran while one was open for 7% of the time, Pallas kernels for 0%

profile of v1, /device:TPU:0, one launch (start us, length us, event | category | flops | bytes accessed | tf_op | source)
XLA Modules:
  0.0 388.4 jit_solution(17129593819143572674)
XLA Ops:
  6.6 1.8 copy.47
  8.5 1.7 copy.49
  10.2 1.8 copy.51
  13.3 7.3 %all-to-all-start = ((s32[8,1,256]{2,1,0:T(1,128)}), s32[8,1,256]{2,1,0:T(1,128)S(1)}, u32[]{:S(2)}, u32[]{:S(2)}) async-start(s32[8,1,256]{2,1,0:T(1,128)} %stack.2), calls=%async_computation | async-start | bytes 16384 | tf_op jit(solution)/shard_map/all_to_all | solution.py:95
  21.7 2.3 reduce-window.6
  26.7 21.0 %all-gather = s32[8,1,256]{2,1,0:T(1,128)S(1)} all-gather(s32[1,1,256]{2,1,0:T(1,128)S(1)} %bitcast.89), channel_id=1, replica_groups=mesh['sp'=8,'tp'=4] {'sp'}, dimensions={0}, use_global_device_ids=true | all-gather | bytes 9216 | tf_op jit(solution)/shard_map/all_gather | solution.py:72
  51.6 40.3 %all-gather.7.cloned.1.call-done = bf16[2048,256]{0,1:T(8,128)(2,1)} async-done(((bf16[256,256]{0,1:T(8,128)(2,1)}), bf16[2048,256]{0,1:T(8,128)(2,1)}) %all-gather.7.cloned.1.call-update) | async-done | bytes 1048592 | tf_op jit(solution)/shard_map/all_gather | solution.py:71
  91.9 12.4 %conditional.2 = (f32[4,256]{1,0:T(4,128)}, f32[4,256]{1,0:T(4,128)S(1)}, f32[4,256]{1,0:T(4,128)}, f32[4,256]{1,0:T(4,128)S(1)}) conditional(s32[]{:T(128)} %convert_element_type.56, () %tuple.24, (s32[256]{0:T(256)S(1)}, s32[2048]{0:T(1024)S(1)}, s32[256]{0:T(256)S(1)}, bf16[2048,256]{0,1:T(8,128)(2,1)}, bf16[256,4,64]{0,2,1:T(8,128)(2,1)S(1)}, ...), branch_computations={%region_2.3_spmd, %region_3.8_spmd} | conditional | flops 571996160 | bytes 50120764 | solution.py:90
  91.9 2.6 fusion.55
  95.1 3.1 fusion.1
  98.8 5.5 %select_reduce_fusion = (f32[4,256]{1,0:T(4,128)S(1)}, f32[4,256]{1,0:T(4,128)S(1)}) fusion(f32[4,256,2048]{2,1,0:T(8,128)S(1)} %get-tuple-element.107, f32[4,256]{1,0:T(4,128)} %get-tuple-element.123, pred[256,2048]{1,0:T(8,128)(4,1)S(1)} %fusion.2, f32[4,256]{1,0:T(4,128)} %get-tuple-element.121, f32[4,256,2048]{2,1,0:T(8,128)S(1)} %fusion.55), kind=kLoop, calls=%fused_computation.2 | loop fusion | flops 20969472 | bytes 17317888 | tf_op jit(solution)/shard_map/cond/branch_1_fun/reduce_sum | solution.py:84
  104.4 39.0 %all-gather.9.cloned.1.call-done = bf16[2048,512]{0,1:T(8,128)(2,1)} async-done(((bf16[256,512]{0,1:T(8,128)(2,1)}), bf16[2048,512]{0,1:T(8,128)(2,1)}) %all-gather.9.cloned.1.call-update) | async-done | bytes 2097168 | tf_op jit(solution)/shard_map/all_gather | solution.py:93
  143.4 16.8 %conditional.3 = (f32[4,256,128]{1,2,0:T(8,128)S(1)}, f32[4,256,1]{1,0,2:T(4,128)S(1)}) conditional(s32[]{:T(128)} %convert_element_type.55, () %tuple.23, (s32[256]{0:T(256)S(1)}, s32[8,1,256]{2,1,0:T(1,128)S(1)}, s32[256]{0:T(256)S(1)}, bf16[2048,256]{0,1:T(8,128)(2,1)}, bf16[256,4,64]{0,2,1:T(8,128)(2,1)S(1)}, /*index=5*/f32[4,256]{1,0:T(4,128)}, ...), branch_computations={%region_8.9_spmd, %region_9.0_spmd} | conditional | flops 1098644480 | bytes 22837280 | solution.py:117
  143.4 5.7 %fusion.56 = f32[4,256,2048]{2,1,0:T(8,128)} fusion(bf16[256,4,64]{0,2,1:T(8,128)(2,1)S(1)} %get-tuple-element.59, bf16[2048,4,64]{0,2,1:T(8,128)(2,1)} %bitcast.76), kind=kOutput, calls=%fused_computation.113 | convolution fusion | flops 268435456 | bytes 9568256 | tf_op jit(solution)/shard_map/cond/branch_1_fun/qhd,khd->hqk/dot_general | solution.py:62
  150.5 9.6 %multiply_reduce_fusion = (f32[4,256]{1,0:T(4,128)S(1)}, f32[4,256,128]{1,2,0:T(8,128)S(1)}) fusion(bf16[2048,4,128]{0,2,1:T(8,128)(2,1)} %bitcast.96, f32[4,256,2048]{2,1,0:T(8,128)} %fusion.56, bf16[256,4,64]{0,2,1:T(8,128)(2,1)S(1)} %get-tuple-element.64, bf16[2048,4,64]{0,2,1:T(8,128)(2,1)} %bitcast.83, f32[4,256]{1,0:T(4,128)S(1)} %get-tuple-element.67, ...), kind=kOutput, calls=%fused_computation.21 | convolution fusion | flops 828636160 | bytes 12734480 | tf_op jit(solution)/shard_map/cond/branch_1_fun/hqk,khv->hqv/dot_general | solution.py:110
  160.3 3.4 convolution_convert_fusion.1
  164.5 33.9 %all-reduce.2.cloned.1.call-done = bf16[256,2048]{1,0:T(8,128)(2,1)} async-done(((bf16[256,2048]{1,0:T(8,128)(2,1)}), bf16[256,2048]{1,0:T(8,128)(2,1)}) %all-reduce.2.cloned.1.call-update) | async-done | bytes 1048592 | tf_op jit(solution)/shard_map/psum | solution.py:125
  198.4 3.1 convert_add_fusion
  202.1 3.3 gather_fusion
  205.4 1.8 broadcast_select_fusion
  207.2 53.2 %all_to_all.16 = bf16[8,64,2048]{2,1,0:T(8,128)(2,1)S(1)} all-to-all(bf16[8,64,2048]{2,1,0:T(8,128)(2,1)S(1)} %broadcast_select_fusion), channel_id=1, replica_groups=mesh['sp'=8,'tp'=4] {'sp'}, dimensions={0} | all-to-all | bytes 4194304 | tf_op jit(solution)/shard_map/all_to_all | solution.py:149
  261.7 2.2 fusion.16
  263.9 6.3 %convolution_convert_fusion = bf16[512,2048]{1,0:T(8,128)(2,1)} fusion(bf16[1,512,2048]{2,1,0:T(8,128)(2,1)S(1)} %copy-done, bf16[512,2048]{1,0:T(8,128)(2,1)} %bitcast.79, bf16[1,2048,512]{2,1,0:T(8,128)(2,1)} %param.37, f32[512,512]{1,0:T(8,128)} %fusion.16), kind=kOutput, calls=%fused_computation.25 | convolution fusion | flops 2150105088 | bytes 9437184 | tf_op jit(solution)/shard_map/dot_general | solution.py:155
  270.2 4.5 %all-to-all-start.2 = ((bf16[8,64,2048]{2,1,0:T(8,128)(2,1)}), bf16[8,64,2048]{2,1,0:T(8,128)(2,1)}, u32[]{:S(2)}, u32[]{:S(2)}) async-start(bf16[8,64,2048]{2,1,0:T(8,128)(2,1)} %bitcast.77), calls=%async_computation.2 | async-start | bytes 4194304 | tf_op jit(solution)/shard_map/all_to_all | solution.py:158
  275.1 1.5 fusion.57
  276.6 45.4 %all-to-all-done.2 = bf16[8,64,2048]{2,1,0:T(8,128)(2,1)} async-done(((bf16[8,64,2048]{2,1,0:T(8,128)(2,1)}), bf16[8,64,2048]{2,1,0:T(8,128)(2,1)}, u32[]{:S(2)}, u32[]{:S(2)}) %all-to-all-start.2) | async-done | bytes 2097184 | tf_op jit(solution)/shard_map/all_to_all | solution.py:158
  322.0 10.7 %gather_fusion.1 = bf16[1024,2048]{1,0:T(8,128)(2,1)} fusion(bf16[512,2048]{1,0:T(8,128)(2,1)} %bitcast.25, s32[1024]{0:T(1024)S(1)} %broadcast_clamp_fusion), kind=kCustom, calls=%fused_computation.1 | custom fusion | bytes 8392704 | tf_op jit(solution)/shard_map/gather | solution.py:166
  332.6 8.3 %reshape.454 = f32[256,4,2048]{2,1,0:T(4,128)} reshape(bf16[1024,2048]{1,0:T(8,128)(2,1)} %gather_fusion.1) | data formatting | bytes 12582912 | tf_op jit(solution)/shard_map/convert_element_type | solution.py:166
  340.9 11.4 %multiply_reduce_fusion.1 = f32[256,2048]{1,0:T(8,128)} fusion(f32[256,4,2048]{2,1,0:T(4,128)} %reshape.454, f32[256,4]{1,0:T(8,128)S(1)} %copy.55), kind=kLoop, calls=%fused_computation.24 | loop fusion | flops 3670016 | bytes 10489856 | tf_op jit(solution)/shard_map/reduce_sum | solution.py:168
  352.4 3.7 fusion.12
  356.1 23.9 %reduce-scatter.2.cloned.1.call-done = bf16[64,2048]{1,0:T(8,128)(2,1)} async-done(((bf16[256,2048]{1,0:T(8,128)(2,1)}), bf16[64,2048]{1,0:T(8,128)(2,1)}) %reduce-scatter.2.cloned.1.call-update) | async-done | bytes 262160 | tf_op jit(solution)/shard_map/reduce_scatter | solution.py:176
  380.0 1.9 add_convert_fusion
  (80 shorter events, 11.7 us)
Async XLA Ops:
  6.5 257.4 %copy-start = (bf16[1,512,2048]{2,1,0:T(8,128)(2,1)S(1)}, bf16[1,512,2048]{2,1,0:T(8,128)(2,1)}, u32[]{:S(2)}) copy-start(bf16[1,512,2048]{2,1,0:T(8,128)(2,1)} %param.38) | copy-start | bytes 6291460
  6.5 18.1 %copy-start.8 = (s32[256]{0:T(256)S(1)}, s32[256]{0:T(256)}, u32[]{:S(2)}) copy-start(s32[256]{0:T(256)} %param.29) | copy-start | bytes 3076
  6.5 18.6 %copy-start.6 = (bf16[256,256]{1,0:T(8,128)(2,1)S(1)}, bf16[256,256]{1,0:T(8,128)(2,1)}, u32[]{:S(2)}) copy-start(bf16[256,256]{1,0:T(8,128)(2,1)} %param.25) | copy-start | bytes 393220
  6.5 18.7 %copy-start.7 = (bf16[256,256]{1,0:T(8,128)(2,1)S(1)}, bf16[256,256]{1,0:T(8,128)(2,1)}, u32[]{:S(2)}) copy-start(bf16[256,256]{1,0:T(8,128)(2,1)} %param.24) | copy-start | bytes 393220
  6.5 45.1 %all-gather.5.cloned.1.call-start = ((), (), s32[]{:S(2)}) async-start(), calls=%async_computation.4 | async-start | bytes 1179648 | tf_op jit(solution)/shard_map/all_gather | solution.py:91
  8.4 83.5 %all-gather.7.cloned.1.call-start = ((), (), s32[]{:S(2)}) async-start(), calls=%async_computation.5 | async-start | bytes 1179648 | tf_op jit(solution)/shard_map/all_gather | solution.py:71
  10.1 133.2 %all-gather.9.cloned.1.call-start = ((), (), s32[]{:S(2)}) async-start(), calls=%async_computation.6 | async-start | bytes 2359296 | tf_op jit(solution)/shard_map/all_gather | solution.py:93
  13.3 36.3 %all-to-all-start = ((s32[8,1,256]{2,1,0:T(1,128)}), s32[8,1,256]{2,1,0:T(1,128)S(1)}, u32[]{:S(2)}, u32[]{:S(2)}) async-start(s32[8,1,256]{2,1,0:T(1,128)} %stack.2), calls=%async_computation | async-start | bytes 16384 | tf_op jit(solution)/shard_map/all_to_all | solution.py:95
  20.6 177.8 %all-reduce.2.cloned.1.call-start = ((), (), s32[]{:S(2)}) async-start(), calls=%async_computation.7 | async-start | bytes 2097152 | tf_op jit(solution)/shard_map/psum | solution.py:125
  91.9 51.5 %copy-start.14 = (f32[4]{0:T(128)S(1)}, f32[4]{0:T(128)}, u32[]{:S(2)}) copy-start(f32[4]{0:T(128)} %param.30) | copy-start | bytes 52
  91.9 3.2 copy-start.5
  143.4 16.8 %copy-start.12 = (f32[128]{0:T(128)S(1)}, f32[128]{0:T(128)}, u32[]{:S(2)}) copy-start(f32[128]{0:T(128)} %param.31) | copy-start | bytes 1540
  160.3 38.1 %copy-start.1 = (bf16[256,2048]{1,0:T(8,128)(2,1)S(1)}, bf16[256,2048]{1,0:T(8,128)(2,1)}, u32[]{:S(2)}) copy-start(bf16[256,2048]{1,0:T(8,128)(2,1)} %param.23) | copy-start | bytes 3145732
  164.5 37.0 %copy-start.10 = (f32[2048]{0:T(1024)S(1)}, f32[2048]{0:T(1024)}, u32[]{:S(2)}) copy-start(f32[2048]{0:T(1024)} %param.33) | copy-start | bytes 24580
  198.4 3.1 copy-start.2
  198.4 3.1 copy-start.3
  207.2 54.5 %copy-start.13 = (bf16[1,2048,512]{2,1,0:T(8,128)(2,1)S(1)}, bf16[1,2048,512]{2,1,0:T(8,128)(2,1)}, u32[]{:S(2)}) copy-start(bf16[1,2048,512]{2,1,0:T(8,128)(2,1)} %param.36) | copy-start | bytes 6291460
  260.4 1.3 copy-start.4
  270.2 4.7 %copy-start.9 = (s32[256,4]{0,1:T(4,128)S(1)}, s32[256,4]{0,1:T(4,128)}, u32[]{:S(2)}) copy-start(s32[256,4]{0,1:T(4,128)} %param.34) | copy-start | bytes 12292
  270.2 4.7 %copy-start.11 = (f32[256,4]{0,1:T(4,128)S(1)}, f32[256,4]{0,1:T(4,128)}, u32[]{:S(2)}) copy-start(f32[256,4]{0,1:T(4,128)} %param.35) | copy-start | bytes 12292
  270.2 51.7 %all-to-all-start.2 = ((bf16[8,64,2048]{2,1,0:T(8,128)(2,1)}), bf16[8,64,2048]{2,1,0:T(8,128)(2,1)}, u32[]{:S(2)}, u32[]{:S(2)}) async-start(bf16[8,64,2048]{2,1,0:T(8,128)(2,1)} %bitcast.77), calls=%async_computation.2 | async-start | bytes 4194304 | tf_op jit(solution)/shard_map/all_to_all | solution.py:158
  274.7 105.2 %reduce-scatter.2.cloned.1.call-start = ((), (), s32[]{:S(2)}) async-start(), calls=%async_computation.8 | async-start | bytes 1310720 | tf_op jit(solution)/shard_map/reduce_scatter | solution.py:176
Sparse Core Ops, SparseCore 0:
  9.4 42.2 all-gather.4
  53.7 38.2 all-gather.6
  94.0 49.3 all-gather.8
  163.9 34.4 all-reduce.1
  356.2 23.7 reduce-scatter.1
